TPU v7x, 32 devices: a whole 2x2x4 slice. The times are simulated.
32 devices in a mesh: sp: 8 (over z, x), tp: 4 (over y, core).
Axes of the slice: x: 2, y: 2, z: 4, core: 2. Of those that a mesh axis runs over, the one named last changes fastest.
Arguments:
- queries: bfloat16 [3072, 1024], P('sp', 'tp'), may hold values from -160 to 160
- key_vectors: bfloat16 [3072, 1024], P('sp', 'tp'), may hold values from -7 to 7
- values: bfloat16 [3072, 1024], P('sp', 'tp'), may hold values from -6 to 6
- head_lambda: float32 [8], P('tp'), may hold values from 0.3 to 0.8
- head_gain: float32 [128], replicated, may hold values from 0.1 to 1.9
- w_out: bfloat16 [1024, 2048], P('tp'), may hold values from -0.1875 to 0.1875
- residual: bfloat16 [3072, 2048], P(('sp', 'tp')), may hold values from -6 to 6
- ffn_gain: float32 [2048], replicated, may hold values from 0.1 to 1.9
- route_ids: int32 [3072, 2], P(('sp', 'tp')), may hold values from 0 to 7, all different within a row; in each aligned block of 96 rows (0 to 95, 96 to 191, ...) at most 30 rows name the same one
- route_logits: float32 [3072, 2], P(('sp', 'tp')), may hold values from -8 to 310
- w_gate: bfloat16 [8, 2048, 2048], P('sp', None, 'tp'), may hold values from -0.3125 to 0.3125
- w_up: bfloat16 [8, 2048, 2048], P('sp', None, 'tp'), may hold values from -0.3125 to 0.3125
- w_down: bfloat16 [8, 2048, 2048], P('sp', 'tp'), may hold values from -0.125 to 0.125
Outputs:
- layer_out: bfloat16 [3072, 2048], P(('sp', 'tp'))
Inputs may be any that keep to these rules, and one draw needn't show every extreme that they name: `route_ids`: in the rows of one device after the attention (aligned blocks of 96 rows) no expert is named by more than 30 rows, a bound that some block reaches while other experts in the same block get fewer rows; each row names 2 different experts.
All inputs are finite; a program needn't handle non-finite values.
Results may differ from a plain program's by a relative error of at most 0.023.
Values may be sent and summed in bfloat16 or wider, within the bound.
A program may use at most 192 MiB of HBM per device.

v0:
```python
import jax
import jax.numpy as jnp
from jax import lax
from jax.sharding import PartitionSpec as P

SEGMENT = 64
SEQUENCES = 1
EPS = 1e-06
NEG = -1e30
CLAMP = 7.0
ALPHA = 1.702
OUT_FACTOR = 0.8


def shards(
    queries,
    key_vectors,
    values,
    head_lambda,
    head_gain,
    w_out,
    residual,
    ffn_gain,
    route_ids,
    route_logits,
    w_gate,
    w_up,
    w_down,
):
    tok_count = queries.shape[0]
    local_heads = head_lambda.shape[0]
    head_width = queries.shape[1] // (2 * local_heads)
    value_width = values.shape[1] // local_heads
    score_scale = head_width ** (-0.5)
    n_tp = lax.axis_size("tp")
    n_sp = lax.axis_size("sp")
    seq_length = tok_count * n_sp // SEQUENCES
    query_pos = lax.axis_index("sp") * tok_count + jnp.arange(tok_count, dtype=jnp.int32)
    query_seg = query_pos // SEGMENT
    query_seq = query_pos // seq_length
    seq_begin = query_seq[0] * seq_length
    last_seg = query_seg[tok_count - 1]
    query_heads = queries.reshape(tok_count, local_heads, 2, head_width)

    def absorb(carry, key_block, value_block, key_start):
        maxima, totals, sums = carry
        block_len = key_block.shape[0]
        key_pos = key_start + jnp.arange(block_len, dtype=jnp.int32)
        visible = ((key_pos // SEGMENT)[None, :] <= query_seg[:, None]) & (
            (key_pos // seq_length)[None, :] == query_seq[:, None]
        )
        score = (
            jnp.einsum(
                "qhjd,khjd->jhqk", query_heads, key_block, preferred_element_type=jnp.float32
            )
            * score_scale
        )
        score = jnp.where(visible, score, NEG)
        new_max = jnp.maximum(maxima, jnp.max(score, axis=-1))
        expo = jnp.where(visible, jnp.exp(score - new_max[..., None]), 0.0)
        factor = jnp.exp(maxima - new_max)
        totals = totals * factor + jnp.sum(expo, axis=-1)
        added = jnp.einsum(
            "jhqk,khd->jqhd",
            expo.astype(jnp.bfloat16),
            value_block,
            preferred_element_type=jnp.float32,
        )
        sums = sums * jnp.transpose(factor, (0, 2, 1))[..., None] + added
        return (new_max, totals, sums)

    def maybe_absorb(carry, key_block, value_block, key_start):
        block_len = key_block.shape[0]
        needed = (key_start // SEGMENT <= last_seg) & (key_start + block_len - 1 >= seq_begin)
        return lax.cond(
            needed,
            lambda inner: absorb(inner, key_block, value_block, key_start),
            lambda inner: inner,
            carry,
        )

    initial = (
        jnp.full((2, local_heads, tok_count), NEG, jnp.float32),
        jnp.zeros((2, local_heads, tok_count), jnp.float32),
        jnp.zeros((2, tok_count, local_heads, value_width), jnp.float32),
    )
    key_piece = lax.all_gather(key_vectors, "sp", axis=0, tiled=True)
    value_piece = lax.all_gather(values, "sp", axis=0, tiled=True)
    piece_len = key_piece.shape[0]
    key_rows = key_piece.reshape(piece_len, local_heads, 2, head_width)
    value_rows = value_piece.reshape(piece_len, local_heads, value_width)
    key_step = 512

    def advance(block_index, inner):
        key_offset = block_index * key_step
        key_block = lax.dynamic_slice_in_dim(key_rows, key_offset, key_step, 0)
        value_block = lax.dynamic_slice_in_dim(value_rows, key_offset, key_step, 0)
        return maybe_absorb(inner, key_block, value_block, key_offset)

    maxima, totals, sums = lax.fori_loop(0, piece_len // key_step, advance, initial)
    attended = sums / jnp.transpose(totals, (0, 2, 1))[..., None]
    diff = attended[0] - head_lambda[None, :, None] * attended[1]
    scale_rows = lax.rsqrt(jnp.mean(diff * diff, axis=-1, keepdims=True) + EPS)
    head_rows = (diff * scale_rows * head_gain * OUT_FACTOR).astype(jnp.bfloat16)
    head_rows = head_rows.reshape(tok_count, local_heads * value_width)
    own_count = tok_count // n_tp
    whole_weight = lax.all_gather(w_out, "tp", axis=0, tiled=True)
    token_heads = lax.all_to_all(head_rows, "tp", split_axis=0, concat_axis=1, tiled=True)
    projected = jnp.dot(token_heads, whole_weight, preferred_element_type=jnp.float32)
    mixed = (residual.astype(jnp.float32) + projected).astype(jnp.bfloat16)
    mixed32 = mixed.astype(jnp.float32)
    normed = (
        mixed32 * lax.rsqrt(jnp.mean(mixed32 * mixed32, axis=-1, keepdims=True) + EPS) * ffn_gain
    ).astype(jnp.bfloat16)
    gates = jax.nn.softmax(route_logits, axis=-1)
    top_count = route_ids.shape[1]
    model_width = normed.shape[1]
    cap_slots = max(2, 5 * top_count * tok_count // (4 * n_tp * n_sp))
    flat_ids = route_ids.reshape(-1)
    chosen = (flat_ids[:, None] == jnp.arange(n_sp, dtype=jnp.int32)[None, :]).astype(jnp.int32)
    earlier = jnp.cumsum(chosen, axis=0) - chosen
    slot_rank = jnp.sum(earlier * chosen, axis=1)
    slot_index = flat_ids * cap_slots + slot_rank
    source_rows = jnp.repeat(normed, top_count, axis=0)
    outgoing = (
        jnp.zeros((n_sp * cap_slots, model_width), jnp.bfloat16).at[slot_index].set(source_rows)
    )
    outgoing = outgoing.reshape(n_sp, cap_slots, model_width)
    arrived = lax.all_to_all(outgoing, "sp", split_axis=0, concat_axis=0, tiled=True)
    senders, slot_count, arrived_width = arrived.shape
    flat_in = arrived.reshape(senders * slot_count, arrived_width)
    piece = lax.all_gather(flat_in, "tp", axis=0, tiled=True)
    gate_pre = jnp.dot(piece, w_gate[0], preferred_element_type=jnp.float32)
    up_pre = jnp.dot(piece, w_up[0], preferred_element_type=jnp.float32)
    gate_cut = jnp.minimum(gate_pre, CLAMP)
    up_cut = jnp.clip(up_pre, -CLAMP, CLAMP)
    active = (gate_cut * jax.nn.sigmoid(ALPHA * gate_cut) * (up_cut + 1.0)).astype(jnp.bfloat16)
    reduced = lax.psum_scatter(
        jnp.dot(active, w_down[0], preferred_element_type=jnp.float32).astype(jnp.bfloat16),
        "tp",
        scatter_dimension=0,
        tiled=True,
    )
    reduced = reduced.reshape(senders, slot_count, arrived_width)
    returned = lax.all_to_all(reduced, "sp", split_axis=0, concat_axis=0, tiled=True)
    picked = returned.reshape(n_sp * cap_slots, model_width)[slot_index].astype(jnp.float32)
    weighted = (picked * gates.reshape(-1)[:, None]).reshape(own_count, top_count, model_width)
    return (mixed32 + jnp.sum(weighted, axis=1)).astype(jnp.bfloat16)


def solution(mesh):
    in_specs = (
        P("sp", "tp"),
        P("sp", "tp"),
        P("sp", "tp"),
        P("tp"),
        P(),
        P("tp", None),
        P(("sp", "tp"), None),
        P(),
        P(("sp", "tp"), None),
        P(("sp", "tp"), None),
        P("sp", None, "tp"),
        P("sp", None, "tp"),
        P("sp", "tp", None),
    )
    out_specs = P(("sp", "tp"), None)
    return jax.shard_map(shards, mesh=mesh, in_specs=in_specs, out_specs=out_specs, check_vma=False)
```

profile of v0, /device:TPU:0, one launch (start us, length us, event | category | flops | bytes accessed | tf_op | source)
XLA Modules:
  0.0 338.7 jit_solution(3574506045380296739)
XLA Ops:
  6.6 1.9 copy.37
  8.6 1.8 copy.39
  10.4 0.7 all-gather.9.cloned.1.call-update
  11.1 0.5 slice.22
  11.6 0.6 slice.21
  12.2 0.2 copy.38
  12.4 0.1 copy.50
  12.6 0.1 eq.45
  12.7 0.6 reduce-window.6
  13.3 0.2 slice_reduce_fusion
  13.6 0.1 copy.49
  13.7 0.1 mul.187
  14.4 0.1 add_bitcast_fusion
  14.6 0.1 broadcast_bitcast_fusion
  14.6 42.0 %all-gather.5.cloned.1.call-done = bf16[3072,256]{0,1:T(8,128)(2,1)} async-done(((bf16[384,256]{0,1:T(8,128)(2,1)}), bf16[3072,256]{0,1:T(8,128)(2,1)}) %all-gather.5.cloned.1.call-update) | async-done | bytes 1572880 | tf_op jit(solution)/shard_map/all_gather | solution.py:87
  56.6 2.7 copy.40
  59.3 42.0 %all-gather.7.cloned.1.call-done = bf16[3072,256]{0,1:T(8,128)(2,1)} async-done(((bf16[384,256]{0,1:T(8,128)(2,1)}), bf16[3072,256]{0,1:T(8,128)(2,1)}) %all-gather.7.cloned.1.call-update) | async-done | bytes 1572880 | tf_op jit(solution)/shard_map/all_gather | solution.py:88
  101.3 2.6 copy.42
  103.9 0.1 broadcast_in_dim.55
  104.0 9.5 %while.24 = (s32[]{:T(128)}, f32[2,2,384]{2,1,0:T(2,128)S(1)}, f32[2,2,384]{2,1,0:T(2,128)S(1)}, f32[2,384,2,128]{3,1,0,2:T(8,128)S(1)}, s32[]{:T(128)}, /*index...) while((s32[]{:T(128)}, f32[2,2,384]{2,1,0:T(2,128)S(1)}, ...), condition=%wide.region_5.6_spmd.clone.clone, body=%wide.region_0.5_spmd.clone.clone.sunk | while | flops 310077472 | bytes 12468234 | solution.py:100
  104.7 4.9 %conditional.4 = ((f32[2,2,384]{2,1,0:T(2,128)S(1)}, f32[2,2,384]{2,1,0:T(2,128)S(1)}, f32[2,384,2,128]{3,1,0,2:T(8,128)S(1)})) conditional(s32[]{:T(128)} %convert_element_type.87, (f32[2,2,384]{2,1,0:T(2,128)S(1)}, f32[2,2,384]{2,1,0:T(2,128)S(1)}, f32[2,384,2,128]{3,1,0,2:T(8,128)S(1)}) %tuple.101, (s32[]{:T(128)}, ...), branch_computations={%region_1.1_spmd, %region_2.4_spmd.clone} | conditional | flops 310070912 | bytes 12456133 | solution.py:75
  104.7 0.1 add_select_fusion.3
  104.9 0.2 compare_and_fusion
  105.1 1.7 fusion.4
  106.8 0.9 fusion.5
  107.7 1.9 fusion.12
  113.4 0.3 broadcast_divide_fusion
  113.7 0.9 copy-done.1
  114.6 0.8 fusion.59
  115.4 0.3 copy.45
  115.7 1.1 squeeze.24
  116.8 1.3 copy.46
  118.1 1.1 squeeze.25
  119.2 0.2 fusion.46
  119.4 0.1 copy.47
  119.6 0.5 mul.176
  120.1 0.3 mul.177
  120.4 1.8 multiply_convert_fusion.2
  122.2 3.4 all-to-all-start
  125.6 7.7 %all-to-all-done = bf16[4,96,256]{2,1,0:T(8,128)(2,1)S(1)} async-done(((bf16[4,96,256]{2,1,0:T(8,128)(2,1)}), bf16[4,96,256]{2,1,0:T(8,128)(2,1)S(1)}, u32[]{:S(2)}, u32[]{:S(2)}) %all-to-all-start) | async-done | bytes 196640 | tf_op jit(solution)/shard_map/all_to_all | solution.py:108
  133.3 4.3 %all-gather.9.cloned.1.call-done = bf16[1024,2048]{1,0:T(8,128)(2,1)} async-done(((bf16[256,2048]{1,0:T(8,128)(2,1)}), bf16[1024,2048]{1,0:T(8,128)(2,1)}) %all-gather.9.cloned.1.call-update) | async-done | bytes 4194320 | tf_op jit(solution)/shard_map/all_gather | solution.py:107
  137.6 3.2 multiply_reduce_fusion.1
  140.9 0.9 copy-done.3
  141.8 0.1 multiply_convert_fusion.1
  141.9 0.5 broadcast_in_dim.57
  142.4 1.2 reshape.176
  143.6 3.3 scatter_custom_fusion
  146.9 1.5 reshape.158
  148.4 45.5 %all_to_all.26 = bf16[8,30,2048]{2,1,0:T(8,128)(2,1)} all-to-all(bf16[8,30,2048]{2,1,0:T(8,128)(2,1)S(1)} %reshape.158), channel_id=1, replica_groups=mesh['sp'=8,'tp'=4] {'sp'}, dimensions={0} | all-to-all | bytes 1966080 | tf_op jit(solution)/shard_map/all_to_all | solution.py:129
  193.9 2.4 reshape.159
  196.4 0.2 reduce-scatter.2.cloned.1.call-start
  196.6 31.4 %all-gather.11.cloned.1.call-done = bf16[960,2048]{1,0:T(8,128)(2,1)} async-done(((bf16[240,2048]{1,0:T(8,128)(2,1)}), bf16[960,2048]{1,0:T(8,128)(2,1)}) %all-gather.11.cloned.1.call-update) | async-done | bytes 3932176 | tf_op jit(solution)/shard_map/all_gather | solution.py:132
  228.0 6.3 %fusion.35 = f32[960,512]{1,0:T(8,128)} fusion(bf16[960,2048]{1,0:T(8,128)(2,1)} %all-gather.11.cloned.1.call-done, bf16[1,2048,512]{2,1,0:T(8,128)(2,1)} %param.28), kind=kOutput, calls=%fused_computation.54 | convolution fusion | flops 2013265920 | bytes 7995392 | tf_op jit(solution)/shard_map/dot_general | solution.py:134
  234.4 9.8 %convolution_convert_fusion = bf16[960,2048]{1,0:T(8,128)(2,1)} fusion(bf16[1,512,2048]{2,1,0:T(8,128)(2,1)S(1)} %copy-done, f32[960,512]{1,0:T(8,128)} %fusion.35, bf16[960,2048]{1,0:T(8,128)(2,1)} %all-gather.11.cloned.1.call-done, bf16[1,2048,512]{2,1,0:T(8,128)(2,1)} %param.27), kind=kOutput, calls=%fused_computation.49 | convolution fusion | flops 4033413120 | bytes 14024704 | tf_op jit(solution)/shard_map/dot_general | solution.py:139
  244.3 43.0 %reduce-scatter.2.cloned.1.call-done = bf16[240,2048]{1,0:T(8,128)(2,1)} async-done(((bf16[960,2048]{1,0:T(8,128)(2,1)}), bf16[240,2048]{1,0:T(8,128)(2,1)}) %reduce-scatter.2.cloned.1.call-update) | async-done | bytes 983056 | tf_op jit(solution)/shard_map/reduce_scatter | solution.py:138
  287.3 2.4 reshape.160
  289.7 5.5 %all-to-all-start.2 = ((bf16[8,30,2048]{2,1,0:T(8,128)(2,1)}), bf16[8,30,2048]{2,1,0:T(8,128)(2,1)}, u32[]{:S(2)}, u32[]{:S(2)}) async-start(bf16[8,30,2048]{2,1,0:T(8,128)(2,1)} %reshape.160), calls=%async_computation.3 | async-start | bytes 2097152 | tf_op jit(solution)/shard_map/all_to_all | solution.py:145
  295.3 0.1 copy.51
  295.4 25.6 %all-to-all-done.2 = bf16[8,30,2048]{2,1,0:T(8,128)(2,1)} async-done(((bf16[8,30,2048]{2,1,0:T(8,128)(2,1)}), bf16[8,30,2048]{2,1,0:T(8,128)(2,1)}, u32[]{:S(2)}, u32[]{:S(2)}) %all-to-all-start.2) | async-done | bytes 983072 | tf_op jit(solution)/shard_map/all_to_all | solution.py:145
  321.0 1.5 reshape.161
  322.5 2.0 gather_fusion
  324.5 3.0 reshape.163
  327.6 3.7 %multiply_reduce_fusion = f32[96,2048]{1,0:T(8,128)S(1)} fusion(f32[96,2,2048]{2,1,0:T(2,128)} %reshape.163, f32[96,2]{1,0:T(8,128)S(1)} %copy.51), kind=kLoop, calls=%fused_computation.59 | loop fusion | flops 589824 | bytes 2360064 | tf_op jit(solution)/shard_map/reduce_sum | solution.py:148
  331.3 0.8 add_convert_fusion
  (95 shorter events, 0.9 us)
Async XLA Ops:
  6.5 227.8 %copy-start = (bf16[1,512,2048]{2,1,0:T(8,128)(2,1)S(1)}, bf16[1,512,2048]{2,1,0:T(8,128)(2,1)}, u32[]{:S(2)}) copy-start(bf16[1,512,2048]{2,1,0:T(8,128)(2,1)} %param.29) | copy-start | bytes 6291460
  6.5 5.7 %copy-start.6 = (bf16[384,256]{1,0:T(8,128)(2,1)S(1)}, bf16[384,256]{1,0:T(8,128)(2,1)}, u32[]{:S(2)}) copy-start(bf16[384,256]{1,0:T(8,128)(2,1)} %param.17) | copy-start | bytes 589828
  6.5 5.9 %copy-start.9 = (s32[96,2]{0,1:T(2,128)S(1)}, s32[96,2]{0,1:T(2,128)}, u32[]{:S(2)}) copy-start(s32[96,2]{0,1:T(2,128)} %param.25) | copy-start | bytes 2308
  6.5 8.0 %copy-start.10 = (f32[2]{0:T(128)S(1)}, f32[2]{0:T(128)}, u32[]{:S(2)}) copy-start(f32[2]{0:T(128)} %param.20) | copy-start | bytes 28
  6.5 8.0 %copy-start.11 = (f32[128]{0:T(128)S(1)}, f32[128]{0:T(128)}, u32[]{:S(2)}) copy-start(f32[128]{0:T(128)} %param.21) | copy-start | bytes 1540
  6.5 50.0 %all-gather.5.cloned.1.call-start = ((), (), s32[]{:S(2)}) async-start(), calls=%async_computation.4 | async-start | bytes 1769472 | tf_op jit(solution)/shard_map/all_gather | solution.py:87
  8.5 92.8 %all-gather.7.cloned.1.call-start = ((), (), s32[]{:S(2)}) async-start(), calls=%async_computation.5 | async-start | bytes 1769472 | tf_op jit(solution)/shard_map/all_gather | solution.py:88
  10.3 127.3 %all-gather.9.cloned.1.call-start = ((), (), s32[]{:S(2)}) async-start(), calls=%async_computation.6 | async-start | bytes 5242880 | tf_op jit(solution)/shard_map/all_gather | solution.py:107
  113.7 0.9 copy-start.1
  115.4 3.8 %copy-start.2 = (f32[2,384,2,128]{3,1,0,2:T(8,128)S(1)}, f32[2,384,2,128]{3,1,0,2:T(8,128)}, u32[]{:S(2)}) copy-start(f32[2,384,2,128]{3,1,0,2:T(8,128)} %copy-done.1) | copy-start | bytes 2359300
  119.2 1.2 copy-start.5
  122.2 11.2 %all-to-all-start = ((bf16[4,96,256]{2,1,0:T(8,128)(2,1)}), bf16[4,96,256]{2,1,0:T(8,128)(2,1)S(1)}, u32[]{:S(2)}, u32[]{:S(2)}) async-start(bf16[4,96,256]{2,1,0:T(8,128)(2,1)} %multiply_convert_fusion.2), calls=%async_computation | async-start | bytes 393216 | tf_op jit(solution)/shard_map/all_to_all | solution.py:108
  125.5 102.5 %all-gather.11.cloned.1.call-start = ((), (), s32[]{:S(2)}) async-start(), calls=%async_computation.7 | async-start | bytes 4915200 | tf_op jit(solution)/shard_map/all_gather | solution.py:132
  137.6 4.1 %copy-start.8 = (f32[2048]{0:T(1024)S(1)}, f32[2048]{0:T(1024)}, u32[]{:S(2)}) copy-start(f32[2048]{0:T(1024)} %param.24) | copy-start | bytes 24580
  140.8 0.9 copy-start.3
  196.4 90.9 %reduce-scatter.2.cloned.1.call-start = ((), (), s32[]{:S(2)}) async-start(), calls=%async_computation.8 | async-start | bytes 4915200 | tf_op jit(solution)/shard_map/reduce_scatter | solution.py:138
  244.2 51.0 %copy-start.7 = (f32[96,2]{0,1:T(2,128)S(1)}, f32[96,2]{0,1:T(2,128)}, u32[]{:S(2)}) copy-start(f32[96,2]{0,1:T(2,128)} %param.26) | copy-start | bytes 2308
  289.7 31.3 %all-to-all-start.2 = ((bf16[8,30,2048]{2,1,0:T(8,128)(2,1)}), bf16[8,30,2048]{2,1,0:T(8,128)(2,1)}, u32[]{:S(2)}, u32[]{:S(2)}) async-start(bf16[8,30,2048]{2,1,0:T(8,128)(2,1)} %reshape.160), calls=%async_computation.3 | async-start | bytes 2097152 | tf_op jit(solution)/shard_map/all_to_all | solution.py:145
  324.5 6.8 %copy-start.4 = (f32[96,2048]{1,0:T(8,128)S(1)}, f32[96,2048]{1,0:T(8,128)}, u32[]{:S(2)}) copy-start(f32[96,2048]{1,0:T(8,128)} %copy-done.3) | copy-start | bytes 2359300
Sparse Core Ops, SparseCore 0:
  9.4 47.1 all-gather.4
  58.6 42.5 all-gather.6
  102.9 34.7 all-gather.8
  196.5 31.4 all-gather.10
  244.4 42.8 reduce-scatter.1
where the time goes:
time: 340 us; the launch traced here: 339 us
  waiting for transfers between devices  197 us (58%)
  blocking collectives  45.5 us (13%)
  local copies, waits for them, and re-layouts  36.4 us (11%)
  matrix products  22.9 us (7%)
  between operations  14.1 us (4%)
  starting transfers between devices  9.27 us (3%)
  other arithmetic  9.27 us (3%)
  loops' own time  4.41 us (1%)
    all_to_all x1, blocking collectives, shards(): lax.all_to_all(outgoing, 'sp', split_axis=0, concat_axis=0, tiled=True)  45.5 us
    reduce_scatter x1, waiting for transfers between devices, shards(): lax.psum_scatter(jnp.dot(active, w_down[0], preferred_element_type=jnp.fl...  43 us
    all_gather x1, waiting for transfers between devices, shards(): value_piece = lax.all_gather(values, 'sp', axis=0, tiled=True)  42 us
    all_gather x1, waiting for transfers between devices, shards(): key_piece = lax.all_gather(key_vectors, 'sp', axis=0, tiled=True)  42 us
    all_gather x1, waiting for transfers between devices, shards(): piece = lax.all_gather(flat_in, 'tp', axis=0, tiled=True)  31.4 us
    all_to_all x1, waiting for transfers between devices, shards(): lax.all_to_all(reduced, 'sp', split_axis=0, concat_axis=0, tiled=True)  25.6 us
    unnamed x31, local copies, waits for them, and re-layouts  11 us
    dot_general x1, matrix products, shards(): jnp.dot(active, w_down[0], preferred_element_type=jnp.float32)  9.84 us
  transfers between devices with their start and end apart: 7, of which 7 were waited for; matrix products, arithmetic and copies ran while one was open for 7% of the time, Pallas kernels for 0%

commit v1 on v0

--- a/solution.py
+++ b/solution.py
@@ -84,8 +84,11 @@
         jnp.zeros((2, local_heads, tok_count), jnp.float32),
         jnp.zeros((2, tok_count, local_heads, value_width), jnp.float32),
     )
-    key_piece = lax.all_gather(key_vectors, "sp", axis=0, tiled=True)
-    value_piece = lax.all_gather(values, "sp", axis=0, tiled=True)
+    key_piece, value_piece = jnp.split(
+        lax.all_gather(jnp.concatenate([key_vectors, values], axis=1), "sp", axis=0, tiled=True),
+        [key_vectors.shape[1]],
+        axis=1,
+    )
     piece_len = key_piece.shape[0]
     key_rows = key_piece.reshape(piece_len, local_heads, 2, head_width)
     value_rows = value_piece.reshape(piece_len, local_heads, value_width)

time: 340 us -> 318 us (0.935)
  waiting for transfers between devices: 197 us -> 168 us
  blocking collectives: 45.5 us -> 51.1 us
    all_gather x2 -> x1, waiting for transfers between devices: 84 us -> 61.2 us  [shards(): lax.all_gather(jnp.concatenate([key_vectors, values], axis=1), 'sp', axis...]
    all_to_all x1, blocking collectives: 45.5 us -> 51.1 us  [shards(): lax.all_to_all(outgoing, 'sp', split_axis=0, concat_axis=0, tiled=True)]
    all_gather x1, waiting for transfers between devices: 4.3 us -> 0.38 us  [shards(): whole_weight = lax.all_gather(w_out, 'tp', axis=0, tiled=True)]
  transfers between devices with their start and end apart: 7 -> 6, of which waited for: 7 -> 6; matrix products, arithmetic and copies ran while one was open for 7% -> 7% of each run, Pallas kernels for 0% -> 0%
where the time goes in v1:
time: 318 us; the launch traced here: 317 us
  waiting for transfers between devices  168 us (53%)
  blocking collectives  51.1 us (16%)
  local copies, waits for them, and re-layouts  37.1 us (12%)
  matrix products  22.9 us (7%)
  between operations  14.1 us (4%)
  other arithmetic  10.1 us (3%)
  starting transfers between devices  9.22 us (3%)
  loops' own time  4.1 us (1%)
    all_gather x1, waiting for transfers between devices, shards(): lax.all_gather(jnp.concatenate([key_vectors, values], axis=1), 'sp', axis...  61.2 us
    all_to_all x1, blocking collectives, shards(): lax.all_to_all(outgoing, 'sp', split_axis=0, concat_axis=0, tiled=True)  51.1 us
    reduce_scatter x1, waiting for transfers between devices, shards(): lax.psum_scatter(jnp.dot(active, w_down[0], preferred_element_type=jnp.fl...  43 us
    all_gather x1, waiting for transfers between devices, shards(): piece = lax.all_gather(flat_in, 'tp', axis=0, tiled=True)  31.4 us
    all_to_all x1, waiting for transfers between devices, shards(): lax.all_to_all(reduced, 'sp', split_axis=0, concat_axis=0, tiled=True)  25.6 us
    dot_general x1, matrix products, shards(): jnp.dot(active, w_down[0], preferred_element_type=jnp.float32)  9.85 us
    unnamed x31, local copies, waits for them, and re-layouts  8.37 us
  transfers between devices with their start and end apart: 6, of which 6 were waited for; matrix products, arithmetic and copies ran while one was open for 7% of the time, Pallas kernels for 0%

profile of v1, /device:TPU:0, one launch (start us, length us, event | category | flops | bytes accessed | tf_op | source)
XLA Modules:
  0.0 317.0 jit_solution(3674973550278679588)
XLA Ops:
  6.6 1.2 copy.37
  7.8 1.1 copy.38
  8.9 0.8 pad_maximum_fusion
  9.8 0.7 all-gather.6.cloned.1.call-update
  10.5 0.6 slice.22
  11.1 0.6 slice.21
  11.7 0.2 copy.39
  11.9 0.1 copy.50
  12.0 0.1 eq.45
  12.2 0.6 reduce-window.6
  12.7 0.2 slice_reduce_fusion
  13.0 0.1 copy.49
  13.1 0.1 mul.187
  13.9 0.1 add_bitcast_fusion
  14.0 0.1 broadcast_bitcast_fusion
  14.1 61.2 %all-gather.4.cloned.1.call-done = bf16[3072,512]{0,1:T(8,128)(2,1)} async-done(((bf16[384,512]{0,1:T(8,128)(2,1)}), bf16[3072,512]{0,1:T(8,128)(2,1)}) %all-gather.4.cloned.1.call-update) | async-done | bytes 3145744 | tf_op jit(solution)/shard_map/all_gather | solution.py:88
  75.3 3.3 %fusion.59 = (bf16[3072,256]{0,1:T(8,128)(2,1)}, bf16[3072,256]{0,1:T(8,128)(2,1)S(1)}) fusion(bf16[3072,512]{0,1:T(8,128)(2,1)} %all-gather.4.cloned.1.call-done), kind=kLoop, calls=%fused_computation.107 | loop fusion | bytes 6291456 | tf_op jit(solution)/shard_map/split | solution.py:87
  78.6 1.3 copy.40
  79.9 2.7 copy.42
  82.6 9.2 %while.24 = (s32[]{:T(128)}, f32[2,2,384]{2,1,0:T(2,128)S(1)}, f32[2,2,384]{2,1,0:T(2,128)S(1)}, f32[2,384,2,128]{3,1,0,2:T(8,128)S(1)}, s32[]{:T(128)}, /*index...) while((s32[]{:T(128)}, f32[2,2,384]{2,1,0:T(2,128)S(1)}, ...), condition=%wide.region_5.6_spmd.clone.clone, body=%wide.region_0.5_spmd.clone.clone.sunk | while | flops 310077472 | bytes 12468234 | solution.py:103
  83.3 4.9 %conditional.4 = ((f32[2,2,384]{2,1,0:T(2,128)S(1)}, f32[2,2,384]{2,1,0:T(2,128)S(1)}, f32[2,384,2,128]{3,1,0,2:T(8,128)S(1)})) conditional(s32[]{:T(128)} %convert_element_type.87, (f32[2,2,384]{2,1,0:T(2,128)S(1)}, f32[2,2,384]{2,1,0:T(2,128)S(1)}, f32[2,384,2,128]{3,1,0,2:T(8,128)S(1)}) %tuple.102, (s32[]{:T(128)}, ...), branch_computations={%region_1.1_spmd, %region_2.4_spmd.clone} | conditional | flops 310070912 | bytes 12456133 | solution.py:75
  83.4 0.1 add_select_fusion.3
  83.5 0.2 compare_and_fusion
  83.7 1.7 fusion.4
  85.5 0.9 fusion.5
  86.4 1.9 fusion.12
  91.8 0.3 broadcast_divide_fusion
  92.1 0.9 copy-done.1
  93.0 0.8 fusion.60
  93.8 0.3 copy.45
  94.1 1.1 squeeze.24
  95.2 1.3 copy.46
  96.5 1.1 squeeze.25
  97.6 0.2 fusion.46
  97.8 0.1 copy.47
  98.0 0.5 mul.176
  98.4 0.3 mul.177
  98.8 1.8 multiply_convert_fusion.2
  100.5 3.4 %all-to-all-start = ((bf16[4,96,256]{2,1,0:T(8,128)(2,1)}), bf16[4,96,256]{2,1,0:T(8,128)(2,1)S(1)}, u32[]{:S(2)}, u32[]{:S(2)}) async-start(bf16[4,96,256]{2,1,0:T(8,128)(2,1)} %multiply_convert_fusion.2), calls=%async_computation | async-start | bytes 393216 | tf_op jit(solution)/shard_map/all_to_all | solution.py:111
  104.0 6.0 %all-to-all-done = bf16[4,96,256]{2,1,0:T(8,128)(2,1)S(1)} async-done(((bf16[4,96,256]{2,1,0:T(8,128)(2,1)}), bf16[4,96,256]{2,1,0:T(8,128)(2,1)S(1)}, u32[]{:S(2)}, u32[]{:S(2)}) %all-to-all-start) | async-done | bytes 196640 | tf_op jit(solution)/shard_map/all_to_all | solution.py:111
  110.0 0.4 all-gather.6.cloned.1.call-done
  110.4 3.2 %multiply_reduce_fusion.1 = (f32[96]{0:T(128)S(1)}, f32[96,2048]{1,0:T(8,128)S(1)}) fusion(bf16[96,1024]{1,0:T(8,128)(2,1)S(1)} %bitcast.79, bf16[1024,2048]{1,0:T(8,128)(2,1)} %all-gather.6.cloned.1.call-done, bf16[96,2048]{1,0:T(8,128)(2,1)} %param.23), kind=kOutput, calls=%fused_computation.62 | convolution fusion | flops 403832736 | bytes 5570944 | tf_op jit(solution)/shard_map/dot_general | solution.py:112
  113.6 0.9 copy-done.3
  114.5 0.1 multiply_convert_fusion.1
  114.7 0.5 broadcast_in_dim.57
  115.1 1.2 reshape.176
  116.3 3.3 %scatter_custom_fusion = bf16[240,2048]{1,0:T(8,128)(2,1)} fusion(s32[192]{0:T(256)S(1)} %bitcast.84, bf16[192,2048]{1,0:T(8,128)(2,1)} %reshape.176, bf16[]{:T(256)} %constant.234.clone.1), kind=kCustom, calls=%fused_computation.63 | custom fusion | bytes 983552 | tf_op jit(solution)/shard_map/scatter | solution.py:129
  119.7 1.5 reshape.158
  121.2 51.1 %all_to_all.26 = bf16[8,30,2048]{2,1,0:T(8,128)(2,1)} all-to-all(bf16[8,30,2048]{2,1,0:T(8,128)(2,1)S(1)} %reshape.158), channel_id=1, replica_groups=mesh['sp'=8,'tp'=4] {'sp'}, dimensions={0} | all-to-all | bytes 1966080 | tf_op jit(solution)/shard_map/all_to_all | solution.py:132
  172.3 2.4 reshape.159
  174.7 0.2 reduce-scatter.2.cloned.1.call-start
  175.0 31.4 %all-gather.8.cloned.1.call-done = bf16[960,2048]{1,0:T(8,128)(2,1)} async-done(((bf16[240,2048]{1,0:T(8,128)(2,1)}), bf16[960,2048]{1,0:T(8,128)(2,1)}) %all-gather.8.cloned.1.call-update) | async-done | bytes 3932176 | tf_op jit(solution)/shard_map/all_gather | solution.py:135
  206.4 6.3 %fusion.35 = f32[960,512]{1,0:T(8,128)} fusion(bf16[960,2048]{1,0:T(8,128)(2,1)} %all-gather.8.cloned.1.call-done, bf16[1,2048,512]{2,1,0:T(8,128)(2,1)} %param.28), kind=kOutput, calls=%fused_computation.54 | convolution fusion | flops 2013265920 | bytes 7995392 | tf_op jit(solution)/shard_map/dot_general | solution.py:137
  212.7 9.8 %convolution_convert_fusion = bf16[960,2048]{1,0:T(8,128)(2,1)} fusion(bf16[1,512,2048]{2,1,0:T(8,128)(2,1)S(1)} %copy-done, f32[960,512]{1,0:T(8,128)} %fusion.35, bf16[960,2048]{1,0:T(8,128)(2,1)} %all-gather.8.cloned.1.call-done, bf16[1,2048,512]{2,1,0:T(8,128)(2,1)} %param.27), kind=kOutput, calls=%fused_computation.49 | convolution fusion | flops 4033413120 | bytes 14024704 | tf_op jit(solution)/shard_map/dot_general | solution.py:142
  222.6 43.0 %reduce-scatter.2.cloned.1.call-done = bf16[240,2048]{1,0:T(8,128)(2,1)} async-done(((bf16[960,2048]{1,0:T(8,128)(2,1)}), bf16[240,2048]{1,0:T(8,128)(2,1)}) %reduce-scatter.2.cloned.1.call-update) | async-done | bytes 983056 | tf_op jit(solution)/shard_map/reduce_scatter | solution.py:141
  265.6 2.4 reshape.160
  268.0 5.5 %all-to-all-start.2 = ((bf16[8,30,2048]{2,1,0:T(8,128)(2,1)}), bf16[8,30,2048]{2,1,0:T(8,128)(2,1)}, u32[]{:S(2)}, u32[]{:S(2)}) async-start(bf16[8,30,2048]{2,1,0:T(8,128)(2,1)} %reshape.160), calls=%async_computation.3 | async-start | bytes 2097152 | tf_op jit(solution)/shard_map/all_to_all | solution.py:148
  273.6 0.1 copy.51
  273.7 25.6 %all-to-all-done.2 = bf16[8,30,2048]{2,1,0:T(8,128)(2,1)} async-done(((bf16[8,30,2048]{2,1,0:T(8,128)(2,1)}), bf16[8,30,2048]{2,1,0:T(8,128)(2,1)}, u32[]{:S(2)}, u32[]{:S(2)}) %all-to-all-start.2) | async-done | bytes 983072 | tf_op jit(solution)/shard_map/all_to_all | solution.py:148
  299.3 1.5 reshape.161
  300.8 2.0 gather_fusion
  302.9 3.0 reshape.163
  305.9 3.7 %multiply_reduce_fusion = f32[96,2048]{1,0:T(8,128)S(1)} fusion(f32[96,2,2048]{2,1,0:T(2,128)} %reshape.163, f32[96,2]{1,0:T(8,128)S(1)} %copy.51), kind=kLoop, calls=%fused_computation.59 | loop fusion | flops 589824 | bytes 2360064 | tf_op jit(solution)/shard_map/reduce_sum | solution.py:151
  309.6 0.8 add_convert_fusion
  (94 shorter events, 0.8 us)
Async XLA Ops:
  6.5 206.2 %copy-start = (bf16[1,512,2048]{2,1,0:T(8,128)(2,1)S(1)}, bf16[1,512,2048]{2,1,0:T(8,128)(2,1)}, u32[]{:S(2)}) copy-start(bf16[1,512,2048]{2,1,0:T(8,128)(2,1)} %param.29) | copy-start | bytes 6291460
  6.5 5.1 %copy-start.6 = (bf16[384,256]{1,0:T(8,128)(2,1)S(1)}, bf16[384,256]{1,0:T(8,128)(2,1)}, u32[]{:S(2)}) copy-start(bf16[384,256]{1,0:T(8,128)(2,1)} %param.17) | copy-start | bytes 589828
  6.5 5.3 %copy-start.9 = (s32[96,2]{0,1:T(2,128)S(1)}, s32[96,2]{0,1:T(2,128)}, u32[]{:S(2)}) copy-start(s32[96,2]{0,1:T(2,128)} %param.25) | copy-start | bytes 2308
  6.5 7.5 %copy-start.10 = (f32[2]{0:T(128)S(1)}, f32[2]{0:T(128)}, u32[]{:S(2)}) copy-start(f32[2]{0:T(128)} %param.20) | copy-start | bytes 28
  6.5 7.5 %copy-start.11 = (f32[128]{0:T(128)S(1)}, f32[128]{0:T(128)}, u32[]{:S(2)}) copy-start(f32[128]{0:T(128)} %param.21) | copy-start | bytes 1540
  6.5 68.7 %all-gather.4.cloned.1.call-start = ((), (), s32[]{:S(2)}) async-start(), calls=%async_computation.4 | async-start | bytes 3538944 | tf_op jit(solution)/shard_map/all_gather | solution.py:88
  9.7 100.7 %all-gather.6.cloned.1.call-start = ((), (), s32[]{:S(2)}) async-start(), calls=%async_computation.5 | async-start | bytes 5242880 | tf_op jit(solution)/shard_map/all_gather | solution.py:110
  92.1 0.9 copy-start.1
  93.8 3.7 %copy-start.2 = (f32[2,384,2,128]{3,1,0,2:T(8,128)S(1)}, f32[2,384,2,128]{3,1,0,2:T(8,128)}, u32[]{:S(2)}) copy-start(f32[2,384,2,128]{3,1,0,2:T(8,128)} %copy-done.1) | copy-start | bytes 2359300
  97.5 1.2 copy-start.5
  100.5 9.5 %all-to-all-start = ((bf16[4,96,256]{2,1,0:T(8,128)(2,1)}), bf16[4,96,256]{2,1,0:T(8,128)(2,1)S(1)}, u32[]{:S(2)}, u32[]{:S(2)}) async-start(bf16[4,96,256]{2,1,0:T(8,128)(2,1)} %multiply_convert_fusion.2), calls=%async_computation | async-start | bytes 393216 | tf_op jit(solution)/shard_map/all_to_all | solution.py:111
  103.9 102.5 %all-gather.8.cloned.1.call-start = ((), (), s32[]{:S(2)}) async-start(), calls=%async_computation.6 | async-start | bytes 4915200 | tf_op jit(solution)/shard_map/all_gather | solution.py:135
  110.4 4.1 %copy-start.8 = (f32[2048]{0:T(1024)S(1)}, f32[2048]{0:T(1024)}, u32[]{:S(2)}) copy-start(f32[2048]{0:T(1024)} %param.24) | copy-start | bytes 24580
  113.6 0.9 copy-start.3
  174.7 90.9 %reduce-scatter.2.cloned.1.call-start = ((), (), s32[]{:S(2)}) async-start(), calls=%async_computation.7 | async-start | bytes 4915200 | tf_op jit(solution)/shard_map/reduce_scatter | solution.py:141
  222.6 51.0 %copy-start.7 = (f32[96,2]{0,1:T(2,128)S(1)}, f32[96,2]{0,1:T(2,128)}, u32[]{:S(2)}) copy-start(f32[96,2]{0,1:T(2,128)} %param.26) | copy-start | bytes 2308
  268.0 31.3 %all-to-all-start.2 = ((bf16[8,30,2048]{2,1,0:T(8,128)(2,1)}), bf16[8,30,2048]{2,1,0:T(8,128)(2,1)}, u32[]{:S(2)}, u32[]{:S(2)}) async-start(bf16[8,30,2048]{2,1,0:T(8,128)(2,1)} %reshape.160), calls=%async_computation.3 | async-start | bytes 2097152 | tf_op jit(solution)/shard_map/all_to_all | solution.py:148
  302.9 6.8 %copy-start.4 = (f32[96,2048]{1,0:T(8,128)S(1)}, f32[96,2048]{1,0:T(8,128)}, u32[]{:S(2)}) copy-start(f32[96,2048]{1,0:T(8,128)} %copy-done.3) | copy-start | bytes 2359300
Sparse Core Ops, SparseCore 0:
  9.9 65.3 all-gather.3
  76.8 33.5 all-gather.5
  174.8 31.4 all-gather.7
  222.7 42.8 reduce-scatter.1
